TPU v7x, 256 devices: a whole 4x4x8 slice. The times are simulated.
256 devices in a mesh: rep: 2 (over z_hi), fs: 16 (over z_lo, x), tp: 8 (over y, core).
Axes of the slice: x: 4, y: 4, z: 8 (z_hi: 2, z_lo: 4; z = z_hi * 4 + z_lo), core: 2. Of those that a mesh axis runs over, the one named last changes fastest.
Arguments:
- tokens: bfloat16 [32, 1024, 2048], P(('rep', 'fs')), may hold values from -6 to 6
- mix_gain: bfloat16 [2048], replicated, may hold values from 0.099609375 to 1.8984375
- value_weight: bfloat16 [2048, 1024], P('fs', 'tp'), may hold values from -0.125 to 0.125
- gate_weight: bfloat16 [2048, 1024], P('fs', 'tp'), may hold values from -0.125 to 0.125
- mix_taps: bfloat16 [31, 1024], P(None, 'tp'), may hold values from -1 to 1
- head_gain: bfloat16 [1024], P('tp'), may hold values from 0.099609375 to 1.8984375
- out_weight: bfloat16 [1024, 2048], P('fs', 'tp'), may hold values from -0.1875 to 0.1875
- ffn_gain: bfloat16 [2048], replicated, may hold values from 0.099609375 to 1.8984375
- ffgate_weight: bfloat16 [2048, 6144], P('fs', 'tp'), may hold values from -0.125 to 0.125
- up_weight: bfloat16 [2048, 6144], P('fs', 'tp'), may hold values from -0.125 to 0.125
- ff_taps: bfloat16 [3, 6144], P(None, 'tp'), may hold values from -3.5 to 3.5
- down_weight: bfloat16 [2048, 6144], P('fs', 'tp'), may hold values from -0.078125 to 0.078125
Outputs:
- layer_out: bfloat16 [32, 1024, 2048], P(('rep', 'fs'), 'tp')
All inputs are finite; a program needn't handle non-finite values.
Results may differ from a plain program's by a relative error of at most 0.01.
Values may be sent and summed in bfloat16 or wider, within the bound.
A program may use at most 64 MiB of HBM per device.

v0:
```python
import jax
import jax.numpy as jnp
from jax import lax
from jax.sharding import PartitionSpec as P

HEAD = 128


norm_floor = 0.01


def in_one_piece(arrays, axis, dim, along):
    both = jnp.concatenate(arrays, axis=along)
    result, at, finished = (lax.all_gather(both, axis, axis=dim, tiled=True), 0, [])
    for a in arrays:
        finished.append(lax.slice_in_dim(result, at, at + a.shape[along], axis=along))
        at += a.shape[along]
    return tuple(finished)


def laid_out(parts, dim):
    lengths = list(parts.shape[1:])
    lengths[dim] *= parts.shape[0]
    return jnp.moveaxis(parts, 0, dim).reshape(lengths)


def sent_to_all(value, axis):
    count = lax.axis_size(axis)
    return lax.all_to_all(
        jnp.broadcast_to(value[None], (count, *value.shape)), axis, 0, 0, tiled=True
    )


def collect(value, axis, dim):
    return laid_out(sent_to_all(value, axis), dim)


def row_norm(floats_in, scales):
    floats = floats_in.astype(jnp.float32)
    scaled = floats * lax.rsqrt(jnp.mean(floats * floats, axis=-1, keepdims=True) + norm_floor)
    return (scaled * scales.astype(jnp.float32)).astype(jnp.bfloat16)


def causal_conv(signal, kernel_taps):
    reach = kernel_taps.shape[0]
    length = signal.shape[0]
    padded = jnp.pad(signal, ((reach - 1, 0), (0, 0)))
    summed = padded[0:length] * kernel_taps[0]
    for offset in range(1, reach):
        summed = summed + padded[offset : offset + length] * kernel_taps[offset]
    return summed


def head_norm(signal, scales):
    length = signal.shape[0]
    grouped = signal.reshape(length, signal.shape[1] // HEAD, HEAD)
    centre = grouped - jnp.mean(grouped, axis=-1, keepdims=True)
    spread = jnp.mean(centre * centre, axis=-1, keepdims=True)
    normal = (centre * lax.rsqrt(spread + norm_floor)).reshape(signal.shape)
    return normal * scales.astype(jnp.float32)


def on_device(
    tokens,
    mix_gain,
    value_weight,
    gate_weight,
    mix_taps,
    head_gain,
    out_weight,
    ffn_gain,
    ffgate_weight,
    up_weight,
    ff_taps,
    down_weight,
):
    sequence = tokens[0]
    value_full, gate_full, out_full = (
        *in_one_piece((value_weight, gate_weight), "fs", 0, 1),
        lax.all_gather(out_weight, "fs", axis=0, tiled=True),
    )
    normed = row_norm(sequence, mix_gain)
    values = jnp.dot(normed, value_full, preferred_element_type=jnp.float32)
    gating = jnp.dot(normed, gate_full, preferred_element_type=jnp.float32)
    glu_out = values * jax.nn.sigmoid(gating)
    mixed_pos = causal_conv(glu_out, mix_taps.astype(jnp.float32))
    head_out = jax.nn.silu(head_norm(mixed_pos, head_gain)).astype(jnp.bfloat16)
    out_cols = out_full.shape[1]
    mixer_sum = jnp.dot(collect(head_out, "tp", 1), out_full, preferred_element_type=jnp.float32)
    own_cols = lax.dynamic_slice_in_dim(sequence, lax.axis_index("tp") * out_cols, out_cols, 1)
    hidden_cols = (own_cols.astype(jnp.float32) + mixer_sum).astype(jnp.bfloat16)
    full_rows = collect(hidden_cols, "tp", 1)
    normed_ffn = row_norm(full_rows, ffn_gain)
    ffgate_full, up_full, down_full = in_one_piece(
        (ffgate_weight, up_weight, down_weight), "fs", 0, 1
    )
    ffgate = jnp.dot(normed_ffn, ffgate_full, preferred_element_type=jnp.float32)
    ff_up = jnp.dot(normed_ffn, up_full, preferred_element_type=jnp.float32)
    product = (jax.nn.silu(causal_conv(ffgate, ff_taps.astype(jnp.float32))) * ff_up).astype(
        jnp.bfloat16
    )
    own_count = sequence.shape[0] // lax.axis_size("tp")
    summed_rows = lax.psum_scatter(
        lax.dot_general(
            product, down_full, (((1,), (1,)), ((), ())), preferred_element_type=jnp.float32
        ).astype(jnp.bfloat16),
        "tp",
        scatter_dimension=0,
        tiled=True,
    ).astype(jnp.float32)
    own_rows = lax.dynamic_slice_in_dim(full_rows, lax.axis_index("tp") * own_count, own_count, 0)
    return (own_rows.astype(jnp.float32) + summed_rows).astype(jnp.bfloat16)[None]


def solution(mesh):
    placed = (
        P(("rep", "fs"), None, None),
        P(),
        P("fs", "tp"),
        P("fs", "tp"),
        P(None, "tp"),
        P("tp"),
        P("fs", "tp"),
        P(),
        P("fs", "tp"),
        P("fs", "tp"),
        P(None, "tp"),
        P("fs", "tp"),
    )
    return jax.shard_map(
        on_device,
        mesh=mesh,
        in_specs=placed,
        out_specs=P(("rep", "fs"), "tp", None),
        check_vma=False,
    )
```

profile of v0, /device:TPU:1, one launch (start us, length us, event | category | flops | bytes accessed | tf_op | source)
XLA Modules:
  0.0 286.3 jit_solution(5631899836314753559)
XLA Ops:
  6.5 0.0 all-gather.3.cloned.1.call-start
  6.5 1.4 pad_maximum_fusion.1
  7.9 0.0 all-gather.3.cloned.1.call-update
  8.0 0.0 all-gather.5.cloned.1.call-start
  8.0 2.0 pad_maximum_fusion
  10.0 0.0 all-gather.5.cloned.1.call-update
  10.0 0.7 convert_element_type.73
  10.7 0.7 convert_element_type.70
  11.4 0.7 convert_element_type.72
  12.1 3.1 %fusion = f32[1024]{0:T(1024)S(1)} fusion(bf16[1,1024,2048]{2,1,0:T(8,128)(2,1)} %param.12), kind=kLoop, calls=%fused_computation.2 | loop fusion | flops 6290432 | bytes 4198400 | tf_op jit(solution)/shard_map/reduce_sum | solution.py:40
  15.2 67.9 %all-gather.3.cloned.1.call-done = bf16[2048,256]{1,0:T(8,128)(2,1)} async-done(((bf16[128,256]{1,0:T(8,128)(2,1)}), bf16[2048,256]{1,0:T(8,128)(2,1)}) %all-gather.3.cloned.1.call-update) | async-done | bytes 1048592 | tf_op jit(solution)/shard_map/all_gather | solution.py:14
  83.1 0.0 copy-start
  83.1 0.0 copy-start.4
  83.1 3.8 %fusion.19 = f32[1024,128]{1,0:T(8,128)S(1)} fusion(bf16[1,1024,2048]{2,1,0:T(8,128)(2,1)} %param.12, f32[2048]{0:T(1024)S(1)} %convert_element_type.70, f32[1024]{0:T(1024)S(1)} %add_rsqrt_fusion.2, bf16[2048,256]{1,0:T(8,128)(2,1)} %all-gather.3.cloned.1.call-done), kind=kOutput, calls=%fused_computation.24 | convolution fusion | flops 545652736 | bytes 5255168 | tf_op jit(solution)/shard_map/dot_general | solution.py:84
  86.9 0.0 copy-done
  86.9 0.1 copy-done.4
  87.0 1.3 convolution_multiply_fusion
  88.4 2.3 fusion.48
  90.7 0.0 copy-start.1
  90.7 0.4 multiply_reduce_fusion.1
  91.1 0.4 multiply_convert_fusion.5
  91.4 0.1 copy.14
  91.6 1.6 broadcast_in_dim.6
  93.2 15.7 %all-to-all-start = ((bf16[8,1024,128]{1,2,0:T(8,128)(2,1)}), bf16[8,1024,128]{1,2,0:T(8,128)(2,1)S(1)}, u32[]{:S(2)}, u32[]{:S(2)}) async-start(bf16[8,1024,128]{1,2,0:T(8,128)(2,1)} %broadcast_in_dim.6), calls=%async_computation | async-start | bytes 4194304 | tf_op jit(solution)/shard_map/all_to_all | solution.py:29
  108.9 0.0 copy-done.1
  108.9 47.2 %all_gather.10 = bf16[1024,256]{1,0:T(8,128)(2,1)S(1)} all-gather(bf16[64,256]{1,0:T(8,128)(2,1)S(1)} %copy-done.1), channel_id=1, replica_groups=mesh['rep'=2,'fs'=16,'tp'=8] {'fs'}, dimensions={0}, use_global_device_ids=true | all-gather | bytes 557056 | tf_op jit(solution)/shard_map/all_gather | solution.py:80
  156.1 0.0 all-to-all-done
  156.1 1.8 fusion.16
  157.9 2.3 broadcast_in_dim.7
  160.2 0.0 copy-start.3
  160.2 0.0 copy-start.2
  160.3 8.9 %all-to-all-start.1 = ((bf16[8,1024,256]{2,1,0:T(8,128)(2,1)}), bf16[8,1024,256]{2,1,0:T(8,128)(2,1)}, u32[]{:S(2)}, u32[]{:S(2)}) async-start(bf16[8,1024,256]{2,1,0:T(8,128)(2,1)} %broadcast_in_dim.7), calls=%async_computation.1 | async-start | bytes 8388608 | tf_op jit(solution)/shard_map/all_to_all | solution.py:29
  169.2 0.0 reduce-scatter.2.cloned.1.call-start
  169.2 0.0 copy-done.3
  169.2 0.0 copy-done.2
  169.3 48.7 %all-to-all-done.1 = bf16[8,1024,256]{2,1,0:T(8,128)(2,1)} async-done(((bf16[8,1024,256]{2,1,0:T(8,128)(2,1)}), bf16[8,1024,256]{2,1,0:T(8,128)(2,1)}, u32[]{:S(2)}, u32[]{:S(2)}) %all-to-all-start.1) | async-done | bytes 4194336 | tf_op jit(solution)/shard_map/all_to_all | solution.py:29
  218.0 4.8 %copy.16 = bf16[8,128,8,256]{3,2,0,1:T(8,128)(2,1)} copy(bf16[8,128,8,256]{3,2,1,0:T(8,128)(2,1)} %bitcast.40) | data formatting | bytes 8388608 | tf_op jit(solution)/shard_map/reshape | solution.py:24
  222.8 3.1 %multiply_reduce_fusion = f32[1024]{0:T(1024)S(1)} fusion(bf16[8,1024,256]{2,1,0:T(8,128)(2,1)} %all-to-all-done.1), kind=kLoop, calls=%fused_computation.6 | loop fusion | flops 6290432 | bytes 4198400 | tf_op jit(solution)/shard_map/reduce_sum | solution.py:40
  225.9 0.0 all-gather.5.cloned.1.call-done
  225.9 6.4 %fusion.6 = f32[1024,768]{1,0:T(8,128)S(1)} fusion(bf16[2048,2304]{1,0:T(8,128)(2,1)} %all-gather.5.cloned.1.call-done, bf16[1024,2048]{1,0:T(8,128)(2,1)} %bitcast.82, f32[2048]{0:T(1024)S(1)} %convert_element_type.79, f32[1024]{0:T(1024)S(1)} %add_rsqrt_fusion), kind=kOutput, calls=%fused_computation.11 | convolution fusion | flops 3229614080 | bytes 10498048 | tf_op jit(solution)/shard_map/dot_general | solution.py:97
  232.4 13.4 %convolution_convert_fusion = bf16[1024,2048]{1,0:T(8,128)(2,1)} fusion(bf16[2048,2304]{1,0:T(8,128)(2,1)} %all-gather.5.cloned.1.call-done, f32[1024,768]{1,0:T(8,128)S(1)} %fusion.6, f32[768]{0:T(1024)S(1)} %get-tuple-element.6, f32[768]{0:T(1024)S(1)} %get-tuple-element.7, f32[768]{0:T(1024)S(1)} %get-tuple-element.5, bf16[1024,2048]{1,0:T(8,128)(2,1)} %bitcast.83, ...), kind=kOutput, calls=%fused_computation.7 | convolution fusion | flops 6461587456 | bytes 17847296 | tf_op jit(solution)/shard_map/dot_general | solution.py:104
  245.7 0.0 reduce-scatter.2.cloned.1.call-update
  245.8 31.9 %reduce-scatter.2.cloned.1.call-done = bf16[128,2048]{1,0:T(8,128)(2,1)} async-done(((bf16[1024,2048]{1,0:T(8,128)(2,1)}), bf16[128,2048]{1,0:T(8,128)(2,1)}) %reduce-scatter.2.cloned.1.call-update) | async-done | bytes 524304 | tf_op jit(solution)/shard_map/reduce_scatter | solution.py:103
  277.6 2.1 fusion.22
  (9 shorter events, 0.1 us)
Async XLA Ops:
  6.5 76.6 %all-gather.3.cloned.1.call-start = ((), (), s32[]{:S(2)}) async-start(), calls=%async_computation.3 | async-start | bytes 1114112 | tf_op jit(solution)/shard_map/all_gather | solution.py:14
  8.0 218.0 %all-gather.5.cloned.1.call-start = ((), (), s32[]{:S(2)}) async-start(), calls=%async_computation.4 | async-start | bytes 10027008 | tf_op jit(solution)/shard_map/all_gather | solution.py:14
  83.1 3.8 %copy-start = (bf16[1,1024,2048]{2,1,0:T(8,128)(2,1)S(1)}, bf16[1,1024,2048]{2,1,0:T(8,128)(2,1)}, u32[]{:S(2)}) copy-start(bf16[1,1024,2048]{2,1,0:T(8,128)(2,1)} %param.12) | copy-start | bytes 12582916
  83.1 3.9 %copy-start.4 = (bf16[2048,256]{1,0:T(8,128)(2,1)S(1)}, bf16[2048,256]{1,0:T(8,128)(2,1)}, u32[]{:S(2)}) copy-start(bf16[2048,256]{1,0:T(8,128)(2,1)} %all-gather.3.cloned.1.call-done) | copy-start | bytes 3145732
  90.7 18.2 %copy-start.1 = (bf16[64,256]{1,0:T(8,128)(2,1)S(1)}, bf16[64,256]{1,0:T(8,128)(2,1)}, u32[]{:S(2)}) copy-start(bf16[64,256]{1,0:T(8,128)(2,1)} %param.18) | copy-start | bytes 98308
  93.2 62.9 %all-to-all-start = ((bf16[8,1024,128]{1,2,0:T(8,128)(2,1)}), bf16[8,1024,128]{1,2,0:T(8,128)(2,1)S(1)}, u32[]{:S(2)}, u32[]{:S(2)}) async-start(bf16[8,1024,128]{1,2,0:T(8,128)(2,1)} %broadcast_in_dim.6), calls=%async_computation | async-start | bytes 4194304 | tf_op jit(solution)/shard_map/all_to_all | solution.py:29
  160.2 9.0 %copy-start.3 = (bf16[2048]{0:T(1024)(128)(2,1)S(1)}, bf16[2048]{0:T(1024)(128)(2,1)}, u32[]{:S(2)}) copy-start(bf16[2048]{0:T(1024)(128)(2,1)} %param.19) | copy-start | bytes 12292
  160.2 9.0 %copy-start.2 = (bf16[3,768]{1,0:T(4,128)(2,1)S(1)}, bf16[3,768]{1,0:T(4,128)(2,1)}, u32[]{:S(2)}) copy-start(bf16[3,768]{1,0:T(4,128)(2,1)} %param.22) | copy-start | bytes 13828
  160.3 57.7 %all-to-all-start.1 = ((bf16[8,1024,256]{2,1,0:T(8,128)(2,1)}), bf16[8,1024,256]{2,1,0:T(8,128)(2,1)}, u32[]{:S(2)}, u32[]{:S(2)}) async-start(bf16[8,1024,256]{2,1,0:T(8,128)(2,1)} %broadcast_in_dim.7), calls=%async_computation.1 | async-start | bytes 8388608 | tf_op jit(solution)/shard_map/all_to_all | solution.py:29
  169.2 108.4 %reduce-scatter.2.cloned.1.call-start = ((), (), s32[]{:S(2)}) async-start(), calls=%async_computation.5 | async-start | bytes 4718592 | tf_op jit(solution)/shard_map/reduce_scatter | solution.py:103
Sparse Core Ops, SparseCore 0:
  9.1 73.9 all-gather.2
  84.9 127.3 all-gather.4
  245.9 31.6 reduce-scatter.1
where the time goes:
time: 289 us; the launch traced here: 286 us
  waiting for transfers between devices  149 us (52%)
  blocking collectives  47.2 us (16%)
  matrix products  26.7 us (9%)
  starting transfers between devices  24.7 us (9%)
  other arithmetic  16.8 us (6%)
  between operations  13.3 us (5%)
  local copies, waits for them, and re-layouts  9.1 us (3%)
    all_gather x2, waiting for transfers between devices, in_one_piece(): lax.all_gather(both, axis, axis=dim, tiled=True)  67.9 us
    all_to_all x2, waiting for transfers between devices, sent_to_all(): lax.all_to_all(jnp.broadcast_to(value[None], (count, *value.shape)), axis...  48.7 us
    all_gather x1, blocking collectives, on_device(): lax.all_gather(out_weight, 'fs', axis=0, tiled=True)  47.2 us
    reduce_scatter x1, waiting for transfers between devices, on_device(): lax.psum_scatter(lax.dot_general(product, down_full, (((1,), (1,)), ((),...  31.9 us
    all_to_all x2, starting transfers between devices, sent_to_all(): lax.all_to_all(jnp.broadcast_to(value[None], (count, *value.shape)), axis...  24.6 us
    dot_general x1, matrix products, on_device(): lax.dot_general(product, down_full, (((1,), (1,)), ((), ())), preferred_e...  13.4 us
    dot_general x1, matrix products, on_device(): jnp.dot(normed_ffn, ffgate_full, preferred_element_type=jnp.float32)  6.41 us
    reduce_sum x2, other arithmetic, row_norm(): jnp.mean(floats * floats, axis=-1, keepdims=True) + norm_floor  6.14 us
  transfers between devices with their start and end apart: 5, of which 3 were waited for; matrix products, arithmetic and copies ran while one was open for 10% of the time, Pallas kernels for 0%

commit v1 on v0

v1 whole, which is shorter than its diff:
```python
import jax
import jax.numpy as jnp
from jax import lax
from jax.experimental import pallas as pl
from jax.experimental.pallas import tpu as pltpu
from jax.sharding import PartitionSpec as P

FLOOR = 0.01
CHUNKS = 4
SIDE = 4
F32 = jnp.float32
BF16 = jnp.bfloat16
NT = (((1,), (1,)), ((), ()))


class Exchange:
    def __init__(self, send_sems, recv_sems):
        self.send_sems, self.recv_sems, self.copies = send_sems, recv_sems, {}

    def send(self, key, src, dst, device):
        at = len(self.copies)
        copy = pltpu.make_async_remote_copy(
            src_ref=src,
            dst_ref=dst,
            send_sem=self.send_sems.at[at],
            recv_sem=self.recv_sems.at[at],
            device_id=device,
            device_id_type=pl.DeviceIdType.MESH,
        )
        copy.start()
        self.copies[key] = copy

    def got(self, key):
        self.copies[key].wait_recv()

    def drain(self):
        for copy in self.copies.values():
            copy.wait_send()


def kernel(
    tok_hbm, mixg, value_hbm, gate_hbm, taps, headg, out_hbm, ffng,
    fg_hbm, fu_hbm, fftaps, down_hbm,
    out_ref,
    tok, nb, vbuf, gbuf, obuf, fgbuf, fubuf, dbuf,
    tapf, fftapf, glu, heads, hid, ffg, act, prod,
    ts2, tsp, tsm, tf, r1p, r1m, r2p, r2m, xsend, xrecv, own, outf,
    send_sems, recv_sems, local_sems,
):
    length = nb.shape[0]
    rows = length // CHUNKS
    model = nb.shape[1]
    width = heads.shape[1] // 8
    cols = hid.shape[1] // 8
    units = ffg.shape[1]
    step = 256

    rep, fs, tp = lax.axis_index("rep"), lax.axis_index("fs"), lax.axis_index("tp")
    z, x = lax.div(fs, SIDE), lax.rem(fs, SIDE)
    y, core = lax.div(tp, 2), lax.rem(tp, 2)

    def around(i, d):
        return lax.rem(i + d + SIDE, SIDE)

    def along_x(d):
        return (rep, z * SIDE + around(x, d), tp)

    def along_z(d):
        at = lax.rem(rep * SIDE + z + d + 2 * SIDE, 2 * SIDE)
        return (lax.div(at, SIDE), lax.rem(at, SIDE) * SIDE + x, tp)

    def along_y(d):
        return (rep, fs, around(y, d) * 2 + core)

    partner = (rep, fs, y * 2 + 1 - core)
    yp, ym = along_y(1), along_y(-1)
    x_ring, z_ring = (along_x(1), along_x(-1)), (along_z(1), along_z(-1))
    first_ring, second_ring = (x_ring, z_ring), (z_ring, x_ring)
    place = (z, x)

    local = {}

    def load(key, src, dst):
        copy = pltpu.make_async_copy(src, dst, local_sems.at[len(local)])
        copy.start()
        local[key] = copy

    load("v", value_hbm, vbuf.at[z, x])
    load("g", gate_hbm, gbuf.at[z, x])
    half_o, half_f = out_hbm.shape[0] // 2, fg_hbm.shape[0] // 2
    quarter = down_hbm.shape[0] // 4
    for c in range(CHUNKS):
        load(("tok", c), tok_hbm.at[0, pl.ds(c * rows, rows)], tok.at[pl.ds(c * rows, rows)])
        if c == 0:
            for u in range(2):
                load(("o", u), out_hbm.at[pl.ds(u * half_o, half_o)], obuf.at[z, x, u])
    for u in range(2):
        load(("G", u), fg_hbm.at[pl.ds(u * half_f, half_f)], fgbuf.at[z, x, u])
        load(("U", u), fu_hbm.at[pl.ds(u * half_f, half_f)], fubuf.at[z, x, u])
        mine = pl.multiple_of(u * half_f + core * quarter, quarter)
        load(("D", u), down_hbm.at[pl.ds(mine, quarter)], dbuf.at[u, z, x, core])

    barrier = pltpu.get_barrier_semaphore()
    peers = (*x_ring, *z_ring, yp, ym, partner)
    for peer in peers:
        pl.semaphore_signal(barrier, inc=1, device_id=peer, device_id_type=pl.DeviceIdType.MESH)

    tapf[pl.ds(0, taps.shape[0])] = taps[...].astype(F32)
    fftapf[pl.ds(0, fftaps.shape[0])] = fftaps[...].astype(F32)
    glu[pl.ds(0, 32)] = jnp.zeros((32, glu.shape[1]), F32)
    ffg[pl.ds(0, 8)] = jnp.zeros((8, units), F32)

    pl.semaphore_wait(barrier, len(peers))
    net = Exchange(send_sems, recv_sems)

    def pick_v(u, zi, xi, h=None):
        ref = (vbuf, gbuf)[u]
        half = value_hbm.shape[0] // 2
        return ref.at[zi, xi] if h is None else ref.at[zi, xi, pl.ds(h * half, half)]

    def pick_of(ref):
        def pick(u, zi, xi, h=None):
            half = ref.shape[3] // 2
            return ref.at[zi, xi, u] if h is None else ref.at[zi, xi, u, pl.ds(h * half, half)]

        return pick

    def pick_d(u, zi, xi, h=None):
        return dbuf.at[u, zi, xi] if h is None else dbuf.at[u, zi, xi, h]

    picks = {"V": pick_v, "O": pick_of(obuf), "G": pick_of(fgbuf), "U": pick_of(fubuf), "D": pick_d}

    def near(n, u, d, h=None):
        if u == 0:
            return picks[n](0, z, around(x, d), h)
        return picks[n](1, around(z, d), x, h)

    def block(n, u, d, h):
        pair = pl.ds(2 * h, 2)
        if u == 0:
            return picks[n](0, around(z, d), pair)
        return picks[n](1, pair, around(x, d))

    def relay(key, ref, device):
        net.send(key, ref, ref, device)

    def s1(n):
        for u in range(2):
            ref = picks[n](u, z, x)
            relay((n, u, 1, "p"), ref, first_ring[u][0])
            relay((n, u, 1, "m"), ref, first_ring[u][1])

    def s2(n):
        for u in range(2):
            net.got((n, u, 1, "p"))
            relay((n, u, 2, "p"), near(n, u, -1, 0), first_ring[u][0])
            net.got((n, u, 1, "m"))
            relay((n, u, 2, "m"), near(n, u, 1, 1), first_ring[u][1])

    def s3(n):
        for u in range(2):
            net.got((n, u, 2, "p"))
            net.got((n, u, 2, "m"))
            plus, minus = second_ring[u]
            relay((n, u, 3, "p0"), block(n, u, 0, 0), plus)
            relay((n, u, 3, "m0"), block(n, u, 0, 1), minus)
            relay((n, u, 3, "p1"), block(n, u, 0, 1), plus)
            relay((n, u, 3, "m1"), block(n, u, 0, 0), minus)

    def s4(n):
        for u in range(2):
            plus, minus = second_ring[u]
            net.got((n, u, 3, "p0"))
            relay((n, u, 4, "p"), block(n, u, -1, 0), plus)
            net.got((n, u, 3, "m0"))
            relay((n, u, 4, "m"), block(n, u, 1, 1), minus)

    def s5(n):
        for u in range(2):
            net.got((n, u, 3, "p1"))
            net.got((n, u, 3, "m1"))

    def s6(n):
        for u in range(2):
            net.got((n, u, 4, "p"))
            net.got((n, u, 4, "m"))

    def chunk_ref(buf, wide, c, d, other=False, h=None):
        owner = around(y, d) * 2 + (1 - core if other else core)
        count = rows if h is None else rows // 2
        start = c * rows + (0 if h is None else h * count)
        return buf.at[pl.ds(start, count), pl.ds(pl.multiple_of(owner * wide, wide), wide)]

    def a1(n, buf, wide, c):
        ref = chunk_ref(buf, wide, c, 0)
        relay((n, c, "p"), ref, yp)
        relay((n, c, "m"), ref, ym)
        relay((n, c, "c"), ref, partner)

    def a2(n, buf, wide, c):
        net.got((n, c, "p"))
        relay((n, c, "pp"), chunk_ref(buf, wide, c, -1, h=0), yp)
        relay((n, c, "cp"), chunk_ref(buf, wide, c, -1), partner)
        net.got((n, c, "m"))
        relay((n, c, "mm"), chunk_ref(buf, wide, c, 1, h=1), ym)
        relay((n, c, "cm"), chunk_ref(buf, wide, c, 1), partner)

    def a3(n, buf, wide, c):
        net.got((n, c, "pp"))
        relay((n, c, "cpp"), chunk_ref(buf, wide, c, 2, h=0), partner)
        net.got((n, c, "mm"))
        relay((n, c, "cmm"), chunk_ref(buf, wide, c, 2, h=1), partner)

    def a4(n, c):
        for k in ("c", "cp", "cm", "cpp", "cmm"):
            net.got((n, c, k))

    def norm(src, gain, c):
        few = 16

        def body(i, _):
            at = pl.ds(pl.multiple_of(c * rows + i * few, few), few)
            value = src[at].astype(F32)
            scale = lax.rsqrt(jnp.mean(value * value, axis=-1, keepdims=True) + FLOOR)
            nb[at] = (value * scale * gain[...].astype(F32)).astype(BF16)
            return 0

        lax.fori_loop(0, rows // few, body, 0)

    def mix(c):
        at = pl.ds(c * rows, rows)
        both = jnp.concatenate(
            [vbuf[...].reshape(model, width), gbuf[...].reshape(model, width)], axis=1
        )
        pair = jnp.dot(nb[at], both, preferred_element_type=F32)
        glu[pl.ds(32 + c * rows, rows)] = pair[:, :width] * jax.nn.sigmoid(pair[:, width:])
        few, count = 64, taps.shape[0]
        lead = 32 - (count - 1)

        def body(i, _):
            base = pl.multiple_of(c * rows + i * few, few)
            total = None
            for r in range(8):
                part = None
                tall = few if r == 0 else few + 8
                for q in range(5):
                    k = 8 * q + r - lead
                    if 0 <= k < count:
                        term = glu[pl.ds(base + 8 * q, tall)] * tapf[pl.ds(k, 1)]
                        part = term if part is None else part + term
                part = part[r : r + few]
                total = part if total is None else total + part
            centre = total - jnp.mean(total, axis=-1, keepdims=True)
            spread = jnp.mean(centre * centre, axis=-1, keepdims=True)
            normal = centre * lax.rsqrt(spread + FLOOR) * headg[...].astype(F32)
            lanes = pl.ds(pl.multiple_of(tp * width, width), width)
            heads[pl.ds(base, few), lanes] = jax.nn.silu(normal).astype(BF16)
            return 0

        lax.fori_loop(0, rows // few, body, 0)

    def hidden(c):
        at = pl.ds(c * rows, rows)
        lanes = pl.ds(pl.multiple_of(tp * cols, cols), cols)
        weight = obuf[...].reshape(heads.shape[1], cols)
        total = jnp.dot(heads[at], weight, preferred_element_type=F32)
        hid[at, lanes] = (tok[at, lanes].astype(F32) + total).astype(BF16)

    def gate(c):
        at = pl.ds(c * rows, rows)

        def body(n, _):
            lanes = pl.ds(pl.multiple_of(n * step, step), step)
            weight = fgbuf[:, :, :, :, lanes].reshape(model, step)
            ffg[pl.ds(8 + c * rows, rows), lanes] = jnp.dot(
                nb[at], weight, preferred_element_type=F32
            )
            few = 32

            def conv(i, _):
                base = pl.multiple_of(c * rows + i * few, few)
                seen = ffg[pl.ds(base, few + 8), lanes]
                total = seen[6 : 6 + few] * fftapf[pl.ds(0, 1), lanes]
                total = total + seen[7 : 7 + few] * fftapf[pl.ds(1, 1), lanes]
                total = total + seen[8 : 8 + few] * fftapf[pl.ds(2, 1), lanes]
                act[pl.ds(base, few), lanes] = jax.nn.silu(total)
                return 0

            lax.fori_loop(0, rows // few, conv, 0)
            return 0

        lax.fori_loop(0, units // step, body, 0)

    def up(c):
        at = pl.ds(c * rows, rows)

        def body(n, _):
            lanes = pl.ds(pl.multiple_of(n * step, step), step)
            weight = fubuf[:, :, :, :, lanes].reshape(model, step)
            wide = jnp.dot(nb[at], weight, preferred_element_type=F32)
            prod[core, at, lanes] = (act[at, lanes] * wide).astype(BF16)
            return 0

        lax.fori_loop(0, units // step, body, 0)
        ref = prod.at[core, at]
        relay(("prod", c), ref, partner)

    offsets = (0, -1, 1, 2)
    half = rows // 2

    def down(b, d):
        zb, xb = around(z, offsets[b]), around(x, offsets[b])
        at = pl.ds(pl.multiple_of(around(y, d) * rows, rows), rows)
        total = None
        for k in range(2):
            weight = jnp.concatenate(
                [
                    dbuf[0, zb, :, k].reshape(SIDE * quarter, units),
                    dbuf[1, :, xb, k].reshape(SIDE * quarter, units),
                ],
                axis=0,
            )
            part = lax.dot_general(prod[k, at], weight, NT, preferred_element_type=F32)
            total = part if total is None else total + part
        return total

    def r1(b):
        ts2[b] = down(b, 2).astype(BF16)
        net.send(("r1", b, "p"), ts2.at[b, pl.ds(0, half)], r1p.at[b], yp)
        net.send(("r1", b, "m"), ts2.at[b, pl.ds(half, half)], r1m.at[b], ym)
        tf[0] = down(b, 1)
        tf[1] = down(b, -1)

    def r2(b):
        top, low = pl.ds(0, half), pl.ds(half, half)
        net.got(("r1", b, "p"))
        tsp[b, top] = (tf[0, top] + r1p[b].astype(F32)).astype(BF16)
        tsp[b, low] = tf[0, low].astype(BF16)
        net.send(("r2", b, "p"), tsp.at[b], r2p.at[b], yp)
        net.got(("r1", b, "m"))
        tsm[b, low] = (tf[1, low] + r1m[b].astype(F32)).astype(BF16)
        tsm[b, top] = tf[1, top].astype(BF16)
        net.send(("r2", b, "m"), tsm.at[b], r2m.at[b], ym)
        tf[2] = down(b, 0)

    def r3(b):
        net.got(("r2", b, "p"))
        net.got(("r2", b, "m"))
        mine = pl.ds(pl.multiple_of(core * half, half), half)
        other = pl.ds(pl.multiple_of((1 - core) * half, half), half)
        xsend[b] = tf[2, other] + r2p[b, other].astype(F32) + r2m[b, other].astype(F32)
        net.send(("r3", b), xsend.at[b], xrecv.at[b], partner)
        own[b] = tf[2, mine] + r2p[b, mine].astype(F32) + r2m[b, mine].astype(F32)

    def r4(b):
        zb, xb = around(z, offsets[b]), around(x, offsets[b])
        net.got(("r3", b))
        mine, other = own[b], xrecv[b]
        low = jnp.where(core == 0, mine, other)
        high = jnp.where(core == 0, other, mine)
        for j in range(SIDE):
            for u in range(2):
                at = (u * SIDE + j) * quarter
                both = jnp.concatenate([low[:, at : at + quarter], high[:, at : at + quarter]], axis=1)
                if u == 0:
                    outf[zb, j, :, pl.ds(0, 2 * quarter)] = both
                else:
                    outf[j, xb, :, pl.ds(2 * quarter, 2 * quarter)] = both

    H = ("H", heads, width)
    I = ("I", hid, cols)

    local["v"].wait()
    local["g"].wait()
    s1("V")
    for u in range(2):
        local[("o", u)].wait()
    s1("O")
    for u in range(2):
        theirs = pl.multiple_of(u * half_f + (1 - core) * quarter, quarter)
        net.send(("d", u), down_hbm.at[pl.ds(theirs, quarter)], dbuf.at[u, z, x, core], partner)
    local[("tok", 0)].wait()
    norm(tok, mixg, 0)
    s2("V")
    local[("tok", 1)].wait()
    norm(tok, mixg, 1)
    s2("O")
    s3("V")
    local[("tok", 2)].wait()
    norm(tok, mixg, 2)
    for u in range(2):
        local[("G", u)].wait()
    s1("G")
    s3("O")
    local[("tok", 3)].wait()
    norm(tok, mixg, 3)
    s4("V")
    s2("G")
    s5("V")
    s6("V")
    mix(0)
    a1(*H, 0)
    s4("O")
    s3("G")
    mix(1)
    a1(*H, 1)
    a2(*H, 0)
    for u in range(2):
        local[("U", u)].wait()
    s1("U")
    mix(2)
    a1(*H, 2)
    a2(*H, 1)
    a3(*H, 0)
    s5("O")
    s6("O")
    mix(3)
    a1(*H, 3)
    a2(*H, 2)
    a3(*H, 1)
    a4("H", 0)
    hidden(0)
    a1(*I, 0)
    a2(*H, 3)
    a3(*H, 2)
    a4("H", 1)
    s4("G")
    hidden(1)
    a1(*I, 1)
    a2(*I, 0)
    s2("U")
    a3(*H, 3)
    a4("H", 2)
    hidden(2)
    a1(*I, 2)
    a2(*I, 1)
    a3(*I, 0)
    s3("U")
    a4("H", 3)
    hidden(3)
    a1(*I, 3)
    a2(*I, 2)
    a3(*I, 1)
    a4("I", 0)
    for u in range(2):
        local[("D", u)].wait()
        net.got(("d", u))
    s1("D")
    norm(hid, ffng, 0)
    s5("G")
    s6("G")
    gate(0)
    a2(*I, 3)
    a3(*I, 2)
    a4("I", 1)
    norm(hid, ffng, 1)
    gate(1)
    s4("U")
    s2("D")
    a3(*I, 3)
    a4("I", 2)
    norm(hid, ffng, 2)
    gate(2)
    a4("I", 3)
    norm(hid, ffng, 3)
    gate(3)
    s3("D")
    s5("U")
    s6("U")
    up(0)
    up(1)
    s4("D")
    up(2)
    up(3)
    for c in range(CHUNKS):
        net.got(("prod", c))
    r1(0)
    r2(0)
    s5("D")
    r1(1)
    r3(0)
    r2(1)
    r1(2)
    r3(1)
    r4(0)
    r2(2)
    s6("D")
    r1(3)
    r3(2)
    r4(1)
    r2(3)
    r4(2)
    r3(3)
    r4(3)
    positions = length // 8
    at = pl.ds(pl.multiple_of(tp * positions, positions), positions)
    for zi in range(SIDE):
        for xi in range(SIDE):
            lanes = pl.ds((zi * SIDE + xi) * 4 * quarter, 4 * quarter)
            total = hid[at, lanes].astype(F32) + outf[zi, xi]
            out_ref[0, :, lanes] = total.astype(BF16)
    net.drain()


def on_device(
    tokens,
    mix_gain,
    value_weight,
    gate_weight,
    mix_taps,
    head_gain,
    out_weight,
    ffn_gain,
    ffgate_weight,
    up_weight,
    ff_taps,
    down_weight,
):
    _, length, model = tokens.shape
    width, cols, units = value_weight.shape[1], out_weight.shape[1], ffgate_weight.shape[1]
    deep, deep_o, deep_d = value_weight.shape[0], out_weight.shape[0], down_weight.shape[0]
    rows, positions, part = length // CHUNKS, length // 8, 2 * deep_d
    vmem = pl.BlockSpec(memory_space=pltpu.VMEM)
    hbm = pl.BlockSpec(memory_space=pl.ANY)
    four = (SIDE, SIDE)
    copies = 256
    scratch = [
        pltpu.VMEM((length, model), BF16),
        pltpu.VMEM((length, model), BF16),
        pltpu.VMEM((*four, deep, width), BF16),
        pltpu.VMEM((*four, deep, width), BF16),
        pltpu.VMEM((*four, 2, deep_o // 2, cols), BF16),
        pltpu.VMEM((*four, 2, deep // 2, units), BF16),
        pltpu.VMEM((*four, 2, deep // 2, units), BF16),
        pltpu.VMEM((2, *four, 2, deep_d // 4, units), BF16),
        pltpu.VMEM((32, width), F32),
        pltpu.VMEM((8, units), F32),
        pltpu.VMEM((32 + length, width), F32),
        pltpu.VMEM((length, 8 * width), BF16),
        pltpu.VMEM((length, 8 * cols), BF16),
        pltpu.VMEM((8 + length, units), F32),
        pltpu.VMEM((length, units), F32),
        pltpu.VMEM((2, length, units), BF16),
        pltpu.VMEM((4, rows, part), BF16),
        pltpu.VMEM((4, rows, part), BF16),
        pltpu.VMEM((4, rows, part), BF16),
        pltpu.VMEM((3, rows, part), F32),
        pltpu.VMEM((4, rows // 2, part), BF16),
        pltpu.VMEM((4, rows // 2, part), BF16),
        pltpu.VMEM((4, rows, part), BF16),
        pltpu.VMEM((4, rows, part), BF16),
        pltpu.VMEM((4, rows // 2, part), F32),
        pltpu.VMEM((4, rows // 2, part), F32),
        pltpu.VMEM((4, rows // 2, part), F32),
        pltpu.VMEM((*four, positions, deep_d), F32),
        pltpu.SemaphoreType.DMA((copies,)),
        pltpu.SemaphoreType.DMA((copies,)),
        pltpu.SemaphoreType.DMA((16,)),
    ]
    return pl.pallas_call(
        kernel,
        out_shape=jax.ShapeDtypeStruct((1, positions, model), BF16),
        in_specs=[hbm, vmem, hbm, hbm, vmem, vmem, hbm, vmem, hbm, hbm, vmem, hbm],
        out_specs=vmem,
        scratch_shapes=scratch,
        compiler_params=pltpu.CompilerParams(
            collective_id=0, has_side_effects=True, vmem_limit_bytes=60 * 1024 * 1024
        ),
        name="layer",
    )(
        tokens,
        mix_gain.reshape(1, -1),
        value_weight,
        gate_weight,
        mix_taps,
        head_gain.reshape(1, -1),
        out_weight,
        ffn_gain.reshape(1, -1),
        ffgate_weight,
        up_weight,
        ff_taps,
        down_weight,
    )


def solution(mesh):
    placed = (
        P(("rep", "fs"), None, None),
        P(),
        P("fs", "tp"),
        P("fs", "tp"),
        P(None, "tp"),
        P("tp"),
        P("fs", "tp"),
        P(),
        P("fs", "tp"),
        P("fs", "tp"),
        P(None, "tp"),
        P("fs", "tp"),
    )
    return jax.shard_map(
        on_device,
        mesh=mesh,
        in_specs=placed,
        out_specs=P(("rep", "fs"), "tp", None),
        check_vma=False,
    )
```

time: 289 us -> 121 us (0.42)
  waiting for transfers between devices: 149 us -> 0 us
  Pallas kernels: 0 us -> 116 us
  blocking collectives: 47.2 us -> 0 us
  matrix products: 26.7 us -> 0 us
  starting transfers between devices: 24.7 us -> 0 us
  other arithmetic: 16.8 us -> 0 us
  between operations: 13.3 us -> 0.01 us
  local copies, waits for them, and re-layouts: 9.1 us -> 4.46 us
    pallas_call x0 -> x1, Pallas kernels: none -> 116 us  [on_device(): pl.pallas_call(kernel, out_shape=jax.ShapeDtypeStruct((1, positions, mode...]
    all_gather x2 -> x0, waiting for transfers between devices: 67.9 us -> none  [in_one_piece(): lax.all_gather(both, axis, axis=dim, tiled=True)]
    all_to_all x2 -> x0, waiting for transfers between devices: 48.7 us -> none  [sent_to_all(): lax.all_to_all(jnp.broadcast_to(value[None], (count, *value.shape)), axis...]
    all_gather x1 -> x0, blocking collectives: 47.2 us -> none  [on_device(): lax.all_gather(out_weight, 'fs', axis=0, tiled=True)]
    reduce_scatter x1 -> x0, waiting for transfers between devices: 31.9 us -> none  [on_device(): lax.psum_scatter(lax.dot_general(product, down_full, (((1,), (1,)), ((),...]
    dot_general x5 -> x0, matrix products: 26.7 us -> none  [the longest x1 13.4 us: on_device(): lax.dot_general(product, down_full, (((1,), (1,)), ((), ())), preferred_e...]
    all_to_all x2 -> x0, starting transfers between devices: 24.6 us -> none  [sent_to_all(): lax.all_to_all(jnp.broadcast_to(value[None], (count, *value.shape)), axis...]
    reduce_sum x4 -> x0, other arithmetic: 8.8 us -> none  [the longest x2 6.14 us: row_norm(): jnp.mean(floats * floats, axis=-1, keepdims=True) + norm_floor]
  transfers between devices with their start and end apart: 5 -> 0, of which waited for: 3 -> 0; matrix products, arithmetic and copies ran while one was open for 10% -> 0% of each run, Pallas kernels for 0% -> 0%
where the time goes in v1:
time: 121 us
  Pallas kernels  116 us (96%)
  local copies, waits for them, and re-layouts  4.46 us (4%)
    pallas_call x1, Pallas kernels, on_device(): pl.pallas_call(kernel, out_shape=jax.ShapeDtypeStruct((1, positions, mode...  116 us

profile of v1, /device:TPU:1, one launch (start us, length us, event | category | flops | bytes accessed | tf_op | source)
XLA Modules:
  0.0 120.7 jit_solution(10399917787727781998)
XLA Ops:
  0.0 1.3 %reshape.9.mixg = bf16[1,2048]{1,0:T(2,128)(2,1)} reshape(bf16[2048]{0:T(1024)(128)(2,1)} %param.13) | data formatting | bytes 8192 | tf_op jit(solution)/shard_map/reshape | solution.py:572
  1.3 1.3 %reshape.11.ffng = bf16[1,2048]{1,0:T(2,128)(2,1)} reshape(bf16[2048]{0:T(1024)(128)(2,1)} %param.19) | data formatting | bytes 8192 | tf_op jit(solution)/shard_map/reshape | solution.py:578
  2.6 116.2 %layer.1 = bf16[1,128,2048]{2,1,0:T(8,128)(2,1)} custom-call(bf16[1,1024,2048]{2,1,0:T(8,128)(2,1)} %tok_hbm.1, bf16[1,2048]{1,0:T(2,128)(2,1)} %reshape.9.mixg, bf16[128,128]{1,0:T(8,128)(2,1)} %value_hbm.1, bf16[128,128]{1,0:T(8,128)(2,1)} %gate_hbm.1, bf16[31,128]{1,0:T(8,128)(2,1)} %taps.1, bf16[1,128]{1,0:T(2,128)(2,1)} %bitcast.1, ...), custom_call_target="tpu_custom_call" | custom-call | tf_op jit(solution)/shard_map/layer/pallas_call | solution.py:560
  118.8 1.9 %copy.14 = bf16[1,128,2048]{2,1,0:T(8,128)(2,1)} copy(bf16[1,128,2048]{2,1,0:T(8,128)(2,1)} %layer.1) | data formatting | bytes 1048576

commit v2 on v1

v2 whole, which is shorter than its diff:
```python
import jax
import jax.numpy as jnp
from jax import lax
from jax.experimental import pallas as pl
from jax.experimental.pallas import tpu as pltpu
from jax.sharding import PartitionSpec as P

FLOOR = 0.01
CHUNKS = 4
SIDE = 4
F32 = jnp.float32
BF16 = jnp.bfloat16
NT = (((1,), (1,)), ((), ()))


SETS = {"V": "x", "U": "x", "O": "y", "D": "y", "G": "z"}
RING = {"H": 1, "I": 1, "r1": 1, "r2": 1}
FAR = {"p": "pp", "m": "mm"}
POOL = 40
RECEIVES = 94


def slot_of(key):
    name = key[0]
    if name in SETS:
        return (SETS[name], *key[1:])
    if name in RING and key[2] != "c":
        return ("ring", key[1], FAR[key[2]] if name == "r2" else key[2])
    return key


class Exchange:
    def __init__(self, send_sems, recv_sems):
        self.send_sems, self.recv_sems, self.copies, self.slots = send_sems, recv_sems, {}, {}
        self.started = []

    def send(self, key, src, dst, device):
        turn = len(self.started)
        if turn >= POOL:
            self.started[turn - POOL].wait_send()
        at = self.slots.setdefault(slot_of(key), len(self.slots))
        copy = pltpu.make_async_remote_copy(
            src_ref=src,
            dst_ref=dst,
            send_sem=self.send_sems.at[turn % POOL],
            recv_sem=self.recv_sems.at[at],
            device_id=device,
            device_id_type=pl.DeviceIdType.MESH,
        )
        copy.start()
        self.started.append(copy)
        self.copies[key] = copy

    def got(self, key):
        self.copies[key].wait_recv()

    def drain(self):
        assert len(self.slots) == RECEIVES, len(self.slots)
        for copy in self.started[-POOL:]:
            copy.wait_send()


def kernel(
    tok_hbm, mixg, value_hbm, gate_hbm, taps, headg, out_hbm, ffng,
    fg_hbm, fu_hbm, fftaps, down_hbm,
    out_ref,
    tok, nb, vbuf, gbuf, obuf, fgbuf, fubuf, dbuf,
    tapf, fftapf, glu, heads, hid, ffg, act, prod,
    ts2, tsp, tsm, tf, r1p, r1m, r2p, r2m, xsend, xrecv, own, outf,
    send_sems, recv_sems, local_sems,
):
    length = nb.shape[0]
    rows = length // CHUNKS
    model = nb.shape[1]
    width = heads.shape[1] // 8
    cols = hid.shape[1] // 8
    units = ffg.shape[1]
    step = 256

    rep, fs, tp = lax.axis_index("rep"), lax.axis_index("fs"), lax.axis_index("tp")
    z, x = lax.div(fs, SIDE), lax.rem(fs, SIDE)
    y, core = lax.div(tp, 2), lax.rem(tp, 2)

    def around(i, d):
        return lax.rem(i + d + SIDE, SIDE)

    def along_x(d):
        return (rep, z * SIDE + around(x, d), tp)

    def along_z(d):
        at = lax.rem(rep * SIDE + z + d + 2 * SIDE, 2 * SIDE)
        return (lax.div(at, SIDE), lax.rem(at, SIDE) * SIDE + x, tp)

    def along_y(d):
        return (rep, fs, around(y, d) * 2 + core)

    partner = (rep, fs, y * 2 + 1 - core)
    yp, ym = along_y(1), along_y(-1)
    x_ring, z_ring = (along_x(1), along_x(-1)), (along_z(1), along_z(-1))
    first_ring, second_ring = (x_ring, z_ring), (z_ring, x_ring)
    place = (z, x)

    barrier = pltpu.get_barrier_semaphore()
    peers = (*x_ring, *z_ring, yp, ym, partner)
    for peer in peers:
        pl.semaphore_signal(barrier, inc=1, device_id=peer, device_id_type=pl.DeviceIdType.MESH)

    local = {}

    def load(key, src, dst):
        copy = pltpu.make_async_copy(src, dst, local_sems.at[len(local)])
        copy.start()
        local[key] = copy

    load("v", value_hbm, vbuf.at[z, x])
    load("g", gate_hbm, gbuf.at[z, x])
    half_o, half_f = out_hbm.shape[0] // 2, fg_hbm.shape[0] // 2
    quarter = down_hbm.shape[0] // 4
    for c in range(CHUNKS):
        load(("tok", c), tok_hbm.at[0, pl.ds(c * rows, rows)], tok.at[pl.ds(c * rows, rows)])
        if c == 0:
            for u in range(2):
                load(("O", u), out_hbm.at[pl.ds(u * half_o, half_o)], obuf.at[z, x, u])
    for u in range(2):
        load(("G", u), fg_hbm.at[pl.ds(u * half_f, half_f)], fgbuf.at[z, x, u])
        load(("U", u), fu_hbm.at[pl.ds(u * half_f, half_f)], fubuf.at[z, x, u])
        mine = pl.multiple_of(u * half_f + core * quarter, quarter)
        load(("D", u), down_hbm.at[pl.ds(mine, quarter)], dbuf.at[u, z, x, core])

    tapf[pl.ds(0, taps.shape[0])] = taps[...].astype(F32)
    fftapf[pl.ds(0, fftaps.shape[0])] = fftaps[...].astype(F32)
    glu[pl.ds(0, 32)] = jnp.zeros((32, glu.shape[1]), F32)
    ffg[pl.ds(0, 8)] = jnp.zeros((8, units), F32)

    net = Exchange(send_sems, recv_sems)

    def pick_v(u, zi, xi, h=None):
        ref = (vbuf, gbuf)[u]
        half = value_hbm.shape[0] // 2
        return ref.at[zi, xi] if h is None else ref.at[zi, xi, pl.ds(h * half, half)]

    def pick_of(ref):
        def pick(u, zi, xi, h=None):
            half = ref.shape[3] // 2
            return ref.at[zi, xi, u] if h is None else ref.at[zi, xi, u, pl.ds(h * half, half)]

        return pick

    def pick_d(u, zi, xi, h=None):
        return dbuf.at[u, zi, xi] if h is None else dbuf.at[u, zi, xi, h]

    picks = {"V": pick_v, "O": pick_of(obuf), "G": pick_of(fgbuf), "U": pick_of(fubuf), "D": pick_d}

    def near(n, u, d, h=None):
        if u == 0:
            return picks[n](0, z, around(x, d), h)
        return picks[n](1, around(z, d), x, h)

    def block(n, u, d, h):
        pair = pl.ds(2 * h, 2)
        if u == 0:
            return picks[n](0, around(z, d), pair)
        return picks[n](1, pair, around(x, d))

    def relay(key, ref, device):
        net.send(key, ref, ref, device)

    def s1(n, u):
        if u == 0 or n in "V":
            ready(*own_blocks[n])
        ref = picks[n](u, z, x)
        relay((n, u, 1, "p"), ref, first_ring[u][0])
        relay((n, u, 1, "m"), ref, first_ring[u][1])

    def s2(n, u):
        net.got((n, u, 1, "p"))
        net.got((n, u, 1, "m"))
        relay((n, u, 2, "p"), near(n, u, -1, 0), first_ring[u][0])
        relay((n, u, 2, "m"), near(n, u, 1, 1), first_ring[u][1])

    def s3(n, u):
        net.got((n, u, 2, "p"))
        net.got((n, u, 2, "m"))
        plus, minus = second_ring[u]
        relay((n, u, 3, "p0"), block(n, u, 0, 0), plus)
        relay((n, u, 3, "m0"), block(n, u, 0, 1), minus)
        relay((n, u, 3, "p1"), block(n, u, 0, 1), plus)
        relay((n, u, 3, "m1"), block(n, u, 0, 0), minus)

    def s4(n, u):
        plus, minus = second_ring[u]
        net.got((n, u, 3, "p0"))
        relay((n, u, 4, "p"), block(n, u, -1, 0), plus)
        net.got((n, u, 3, "m0"))
        relay((n, u, 4, "m"), block(n, u, 1, 1), minus)

    def s5(n, u):
        net.got((n, u, 3, "p1"))
        net.got((n, u, 3, "m1"))

    def s6(n, u):
        net.got((n, u, 4, "p"))
        net.got((n, u, 4, "m"))

    def chunk_ref(buf, wide, c, d, h=None):
        count = rows if h is None else rows // 2
        start = c * rows + (0 if h is None else h * count)
        lane = pl.multiple_of(core * SIDE * wide + around(y, d) * wide, wide)
        return buf.at[pl.ds(start, count), pl.ds(lane, wide)]

    def a1(n, buf, wide, c):
        ref = chunk_ref(buf, wide, c, 0)
        relay((n, c, "p"), ref, yp)
        relay((n, c, "m"), ref, ym)

    def a2(n, buf, wide, c):
        net.got((n, c, "p"))
        net.got((n, c, "m"))
        relay((n, c, "pp"), chunk_ref(buf, wide, c, -1, h=0), yp)
        relay((n, c, "mm"), chunk_ref(buf, wide, c, 1, h=1), ym)

    def a3(n, buf, wide, c):
        net.got((n, c, "pp"))
        net.got((n, c, "mm"))
        lane = pl.multiple_of(core * SIDE * wide, SIDE * wide)
        relay((n, c, "c"), buf.at[pl.ds(c * rows, rows), pl.ds(lane, SIDE * wide)], partner)

    def a4(n, c):
        net.got((n, c, "c"))

    def norm(src, gain, c, starts):
        few, wide = 16, model // len(starts)

        def body(i, _):
            at = pl.ds(pl.multiple_of(c * rows + i * few, few), few)
            parts = [src[at, pl.ds(start, wide)] for start in starts]
            value = jnp.concatenate(parts, axis=1).astype(F32)
            scale = lax.rsqrt(jnp.mean(value * value, axis=-1, keepdims=True) + FLOOR)
            nb[at] = (value * scale * gain[...].astype(F32).reshape(1, model)).astype(BF16)
            return 0

        lax.fori_loop(0, rows // few, body, 0, unroll=4)

    def mixa(c):
        at = pl.ds(c * rows, rows)
        both = jnp.concatenate(
            [vbuf[...].reshape(model, width), gbuf[...].reshape(model, width)], axis=1
        )
        pair = jnp.dot(nb[at], both, preferred_element_type=F32)
        glu[pl.ds(32 + c * rows, rows)] = pair[:, :width] * jax.nn.sigmoid(pair[:, width:])

    def mix(c):
        few, count = 64, taps.shape[0]
        lead = 32 - (count - 1)

        def body(i, _):
            base = pl.multiple_of(c * rows + i * few, few)
            total = None
            for r in range(8):
                part = None
                tall = few if r == 0 else few + 8
                for q in range(5):
                    k = 8 * q + r - lead
                    if 0 <= k < count:
                        term = glu[pl.ds(base + 8 * q, tall)] * tapf[pl.ds(k, 1)]
                        part = term if part is None else part + term
                part = part[r : r + few]
                total = part if total is None else total + part
            centre = total - jnp.mean(total, axis=-1, keepdims=True)
            spread = jnp.mean(centre * centre, axis=-1, keepdims=True)
            normal = centre * lax.rsqrt(spread + FLOOR) * headg[...].astype(F32)
            lanes = pl.ds(pl.multiple_of(core * SIDE * width + y * width, width), width)
            heads[pl.ds(base, few), lanes] = jax.nn.silu(normal).astype(BF16)
            return 0

        lax.fori_loop(0, rows // few, body, 0)

    def hidden(c):
        at = pl.ds(c * rows, rows)
        lanes = pl.ds(pl.multiple_of(tp * cols, cols), cols)
        mine = pl.ds(pl.multiple_of(core * SIDE * cols + y * cols, cols), cols)
        weight = jnp.concatenate(
            [obuf[:, 2 * k : 2 * k + 2].reshape(SIDE * width, cols) for k in range(2)], axis=0
        )
        total = jnp.dot(heads[at], weight, preferred_element_type=F32)
        hid[at, mine] = (tok[at, lanes].astype(F32) + total).astype(BF16)

    def gate(c, n):
        at, lanes = pl.ds(c * rows, rows), pl.ds(n * step, step)
        weight = fgbuf[:, :, :, :, lanes].reshape(model, step)
        ffg[pl.ds(8 + c * rows, rows), lanes] = jnp.dot(nb[at], weight, preferred_element_type=F32)
        few = 32
        for i in range(rows // few):
            base = c * rows + i * few
            seen = ffg[pl.ds(base, few + 8), lanes]
            total = seen[6 : 6 + few] * fftapf[pl.ds(0, 1), lanes]
            total = total + seen[7 : 7 + few] * fftapf[pl.ds(1, 1), lanes]
            total = total + seen[8 : 8 + few] * fftapf[pl.ds(2, 1), lanes]
            act[pl.ds(base, few), lanes] = jax.nn.silu(total)

    def up(d, n):
        at = pl.ds(pl.multiple_of(around(y, d) * rows, rows), rows)
        lanes = pl.ds(n * step, step)
        weight = fubuf[:, :, :, :, lanes].reshape(model, step)
        wide = jnp.dot(nb[at], weight, preferred_element_type=F32)
        prod[core, at, lanes] = (act[at, lanes] * wide).astype(BF16)
        if n == units // step - 1:
            relay(("prod", d), prod.at[core, at], partner)

    def up_in(d):
        net.got(("prod", d))

    offsets = (0, -1, 1, 2)
    half = rows // 2

    def down(b, d):
        zb, xb = around(z, offsets[b]), around(x, offsets[b])
        at = pl.ds(pl.multiple_of(around(y, d) * rows, rows), rows)
        total = None
        for k in range(2):
            weight = jnp.concatenate(
                [
                    dbuf[0, zb, :, k].reshape(SIDE * quarter, units),
                    dbuf[1, :, xb, k].reshape(SIDE * quarter, units),
                ],
                axis=0,
            )
            part = lax.dot_general(prod[k, at], weight, NT, preferred_element_type=F32)
            total = part if total is None else total + part
        return total

    def ra(b):
        ts2[b] = down(b, 2).astype(BF16)
        net.send(("r1", b, "p"), ts2.at[b, pl.ds(0, half)], r1p.at[b], yp)
        net.send(("r1", b, "m"), ts2.at[b, pl.ds(half, half)], r1m.at[b], ym)

    def rb(b):
        tf[b, 0] = down(b, 1)
        tf[b, 1] = down(b, -1)

    def rc(b):
        top, low = pl.ds(0, half), pl.ds(half, half)
        net.got(("r1", b, "p"))
        net.got(("r1", b, "m"))
        tsp[b, top] = (tf[b, 0, top] + r1p[b].astype(F32)).astype(BF16)
        tsp[b, low] = tf[b, 0, low].astype(BF16)
        net.send(("r2", b, "p"), tsp.at[b], r2p.at[b], yp)
        tsm[b, low] = (tf[b, 1, low] + r1m[b].astype(F32)).astype(BF16)
        tsm[b, top] = tf[b, 1, top].astype(BF16)
        net.send(("r2", b, "m"), tsm.at[b], r2m.at[b], ym)

    def rd(b):
        tf[b, 2] = down(b, 0)

    def re(b):
        net.got(("r2", b, "p"))
        net.got(("r2", b, "m"))
        mine = pl.ds(pl.multiple_of(core * half, half), half)
        other = pl.ds(pl.multiple_of((1 - core) * half, half), half)
        xsend[b] = tf[b, 2, other] + r2p[b, other].astype(F32) + r2m[b, other].astype(F32)
        net.send(("r3", b), xsend.at[b], xrecv.at[b], partner)
        own[b] = tf[b, 2, mine] + r2p[b, mine].astype(F32) + r2m[b, mine].astype(F32)

    def rf(b):
        zb, xb = around(z, offsets[b]), around(x, offsets[b])
        net.got(("r3", b))
        mine, other = own[b], xrecv[b]
        low = jnp.where(core == 0, mine, other)
        high = jnp.where(core == 0, other, mine)
        for j in range(SIDE):
            for u in range(2):
                at = (u * SIDE + j) * quarter
                both = jnp.concatenate([low[:, at : at + quarter], high[:, at : at + quarter]], axis=1)
                if u == 0:
                    outf[zb, j, :, pl.ds(0, 2 * quarter)] = both
                else:
                    outf[j, xb, :, pl.ds(2 * quarter, 2 * quarter)] = both

    H = ("H", heads, width)
    own_blocks = {
        "V": ("v", "g"),
        **{n: ((n, 0), (n, 1)) for n in "OGUD"},
    }
    in_order = [(t % 2) * SIDE * cols + (t // 2) * cols for t in range(8)]
    I = ("I", hid, cols)

    def ready(*keys):
        for key in keys:
            if key in local:
                local.pop(key).wait()

    def halves():
        for u in range(2):
            theirs = pl.multiple_of(u * half_f + (1 - core) * quarter, quarter)
            net.send(("d", u), down_hbm.at[pl.ds(theirs, quarter)], dbuf.at[u, z, x, core], partner)

    def halves_in():
        for u in range(2):
            net.got(("d", u))

    def normed(c):
        ready(("tok", c))
        norm(tok, mixg, c, [0])

    def renormed(c):
        norm(hid, ffng, c, in_order)

    def meet():
        pl.semaphore_wait(barrier, len(peers))

    for step_of, *given in (
        (normed, 0), (normed, 1), (meet,), (s1, "V", 0), (s1, "V", 1), (halves,), (halves_in,),
        (normed, 2), (normed, 3), (s2, "V", 0), (s2, "V", 1), (s1, "O", 0), (s1, "O", 1), (s1, "G", 0),
        (s1, "G", 1), (s3, "V", 0), (s3, "V", 1), (s2, "O", 0), (s2, "O", 1), (s2, "G", 0), (s2, "G", 1),
        (s4, "V", 0), (s4, "V", 1), (s5, "V", 0), (s5, "V", 1), (s3, "O", 0), (s3, "O", 1), (s3, "G", 0),
        (s3, "G", 1), (s6, "V", 0), (s6, "V", 1), (s1, "U", 0), (s1, "U", 1), (mixa, 0), (mix, 0),
        (a1, *H, 0), (s4, "O", 0), (s4, "O", 1), (s5, "O", 0), (s5, "O", 1), (mixa, 1), (mix, 1),
        (a1, *H, 1), (mixa, 2), (mix, 2), (a1, *H, 2), (mixa, 3), (s4, "G", 0), (s4, "G", 1), (mix, 3),
        (a2, *H, 0), (a1, *H, 3), (a2, *H, 1), (a2, *H, 2), (s5, "G", 0), (s5, "G", 1), (a3, *H, 0),
        (a2, *H, 3), (a4, "H", 0), (s2, "U", 0), (s2, "U", 1), (a3, *H, 1), (s6, "O", 0), (s6, "O", 1),
        (s1, "D", 0), (s1, "D", 1), (hidden, 0), (a3, *H, 2), (a1, *I, 0), (a4, "H", 1), (hidden, 1),
        (a1, *I, 1), (a4, "H", 2), (hidden, 2), (a3, *H, 3), (a4, "H", 3), (hidden, 3), (s6, "G", 0),
        (s6, "G", 1), (s3, "U", 0), (s3, "U", 1), (a2, *I, 0), (a1, *I, 2), (s2, "D", 0), (s2, "D", 1),
        (a2, *I, 1), (a1, *I, 3), (a3, *I, 0), (a4, "I", 0), (renormed, 0), (s4, "U", 0), (s4, "U", 1),
        (gate, 0, 0), (a2, *I, 2), (gate, 0, 1), (gate, 0, 2), (a3, *I, 1), (s5, "U", 0), (s5, "U", 1),
        (a4, "I", 1), (renormed, 1), (a2, *I, 3), (gate, 1, 0), (s3, "D", 0), (s3, "D", 1), (gate, 1, 1),
        (a3, *I, 2), (gate, 1, 2), (a4, "I", 2), (renormed, 2), (gate, 2, 0), (a3, *I, 3), (s6, "U", 0),
        (s6, "U", 1), (gate, 2, 1), (gate, 2, 2), (a4, "I", 3), (renormed, 3), (gate, 3, 0), (gate, 3, 1),
        (gate, 3, 2), (s4, "D", 0), (s4, "D", 1), (up, 2, 0), (up, 2, 1), (up, 2, 2), (up, 1, 0),
        (up, 1, 1), (up, 1, 2), (up, -1, 0), (up_in, 2), (ra, 0), (s5, "D", 0), (s5, "D", 1), (ra, 1),
        (ra, 2), (up_in, 1), (up, -1, 1), (up, -1, 2), (up, 0, 0), (up, 0, 1), (up, 0, 2), (up_in, -1),
        (rb, 0), (s6, "D", 0), (s6, "D", 1), (rc, 0), (ra, 3), (rb, 1), (up_in, 0), (rc, 1), (rd, 0),
        (rd, 1), (rb, 2), (rc, 2), (rd, 2), (rb, 3), (rd, 3), (re, 0), (rc, 3), (rf, 0), (re, 1), (rf, 1),
        (re, 2), (rf, 2), (re, 3), (rf, 3),
    ):
        tag = "_".join(str(part) for part in given if isinstance(part, (int, str)))
        with jax.named_scope(step_of.__name__ + "_" + tag):
            step_of(*given)
    positions = length // 8
    at = pl.ds(pl.multiple_of(tp * positions, positions), positions)
    with jax.named_scope("result"):
        for zi in range(SIDE):
            for xi in range(SIDE):
                lanes = pl.ds((zi * SIDE + xi) * 4 * quarter, 4 * quarter)
                start = in_order[2 * zi + xi // 2] + (xi % 2) * 4 * quarter
                total = hid[at, pl.ds(start, 4 * quarter)].astype(F32) + outf[zi, xi]
                out_ref[0, :, lanes] = total.astype(BF16)
    with jax.named_scope("drain"):
        net.drain()


def on_device(
    tokens,
    mix_gain,
    value_weight,
    gate_weight,
    mix_taps,
    head_gain,
    out_weight,
    ffn_gain,
    ffgate_weight,
    up_weight,
    ff_taps,
    down_weight,
):
    _, length, model = tokens.shape
    width, cols, units = value_weight.shape[1], out_weight.shape[1], ffgate_weight.shape[1]
    deep, deep_o, deep_d = value_weight.shape[0], out_weight.shape[0], down_weight.shape[0]
    rows, positions, part = length // CHUNKS, length // 8, 2 * deep_d
    vmem = pl.BlockSpec(memory_space=pltpu.VMEM)
    hbm = pl.BlockSpec(memory_space=pl.ANY)
    four = (SIDE, SIDE)
    scratch = [
        pltpu.VMEM((length, model), BF16),
        pltpu.VMEM((length, model), BF16),
        pltpu.VMEM((*four, deep, width), BF16),
        pltpu.VMEM((*four, deep, width), BF16),
        pltpu.VMEM((*four, 2, deep_o // 2, cols), BF16),
        pltpu.VMEM((*four, 2, deep // 2, units), BF16),
        pltpu.VMEM((*four, 2, deep // 2, units), BF16),
        pltpu.VMEM((2, *four, 2, deep_d // 4, units), BF16),
        pltpu.VMEM((32, width), F32),
        pltpu.VMEM((8, units), F32),
        pltpu.VMEM((32 + length, width), F32),
        pltpu.VMEM((length, 8 * width), BF16),
        pltpu.VMEM((length, 8 * cols), BF16),
        pltpu.VMEM((8 + length, units), F32),
        pltpu.VMEM((length, units), F32),
        pltpu.VMEM((2, length, units), BF16),
        pltpu.VMEM((4, rows, part), BF16),
        pltpu.VMEM((4, rows, part), BF16),
        pltpu.VMEM((4, rows, part), BF16),
        pltpu.VMEM((4, 3, rows, part), F32),
        pltpu.VMEM((4, rows // 2, part), BF16),
        pltpu.VMEM((4, rows // 2, part), BF16),
        pltpu.VMEM((4, rows, part), BF16),
        pltpu.VMEM((4, rows, part), BF16),
        pltpu.VMEM((4, rows // 2, part), F32),
        pltpu.VMEM((4, rows // 2, part), F32),
        pltpu.VMEM((4, rows // 2, part), F32),
        pltpu.VMEM((*four, positions, deep_d), F32),
        pltpu.SemaphoreType.DMA((POOL,)),
        pltpu.SemaphoreType.DMA((RECEIVES,)),
        pltpu.SemaphoreType.DMA((14,)),
    ]
    return pl.pallas_call(
        kernel,
        out_shape=jax.ShapeDtypeStruct((1, positions, model), BF16),
        in_specs=[hbm, vmem, hbm, hbm, vmem, vmem, hbm, vmem, hbm, hbm, vmem, hbm],
        out_specs=vmem,
        scratch_shapes=scratch,
        compiler_params=pltpu.CompilerParams(
            collective_id=0, has_side_effects=True, vmem_limit_bytes=60 * 1024 * 1024
        ),
        name="layer",
    )(
        tokens,
        mix_gain,
        value_weight,
        gate_weight,
        mix_taps,
        head_gain.reshape(1, -1),
        out_weight,
        ffn_gain,
        ffgate_weight,
        up_weight,
        ff_taps,
        down_weight,
    )


def solution(mesh):
    placed = (
        P(("rep", "fs"), None, None),
        P(),
        P("fs", "tp"),
        P("fs", "tp"),
        P(None, "tp"),
        P("tp"),
        P("fs", "tp"),
        P(),
        P("fs", "tp"),
        P("fs", "tp"),
        P(None, "tp"),
        P("fs", "tp"),
    )
    return jax.shard_map(
        on_device,
        mesh=mesh,
        in_specs=placed,
        out_specs=P(("rep", "fs"), "tp", None),
        check_vma=False,
    )
```

time: 121 us -> 95.3 us (0.79)
  Pallas kernels: 116 us -> 93.2 us
  local copies, waits for them, and re-layouts: 4.46 us -> 1.88 us
    pallas_call x1, Pallas kernels: 116 us -> 93.2 us  [on_device(): pl.pallas_call(kernel, out_shape=jax.ShapeDtypeStruct((1, positions, mode...]
    reshape x2 -> x0, local copies, waits for them, and re-layouts: 2.57 us -> none  [the longest x1 1.29 us: on_device(): mix_gain.reshape(1, -1)]
where the time goes in v2:
time: 95.3 us; the launch traced here: 95.1 us
  Pallas kernels  93.2 us (98%)
  local copies, waits for them, and re-layouts  1.88 us (2%)
    pallas_call x1, Pallas kernels, on_device(): pl.pallas_call(kernel, out_shape=jax.ShapeDtypeStruct((1, positions, mode...  93.2 us

profile of v2, /device:TPU:1, one launch (start us, length us, event | category | flops | bytes accessed | tf_op | source)
XLA Modules:
  0.0 95.1 jit_solution(870523729992458113)
XLA Ops:
  0.0 93.2 %layer.1 = bf16[1,128,2048]{2,1,0:T(8,128)(2,1)} custom-call(bf16[1,1024,2048]{2,1,0:T(8,128)(2,1)} %tok_hbm.1, bf16[2048]{0:T(1024)(128)(2,1)} %mixg.1, bf16[128,128]{1,0:T(8,128)(2,1)} %value_hbm.1, bf16[128,128]{1,0:T(8,128)(2,1)} %gate_hbm.1, bf16[31,128]{1,0:T(8,128)(2,1)} %taps.1, bf16[1,128]{1,0:T(2,128)(2,1)} %bitcast.1, bf16[64,256]{1,0:T(8,128)(2,1)} %out_hbm.1, ...), custom_call_target="tpu_custom_call" | custom-call | tf_op jit(solution)/shard_map/layer/pallas_call | solution.py:506
  93.2 1.9 %copy.14 = bf16[1,128,2048]{2,1,0:T(8,128)(2,1)} copy(bf16[1,128,2048]{2,1,0:T(8,128)(2,1)} %layer.1) | data formatting | bytes 1048576

commit v3 on v2

--- a/solution.py
+++ b/solution.py
@@ -6,7 +6,7 @@
 from jax.sharding import PartitionSpec as P
 
 FLOOR = 0.01
-CHUNKS = 4
+SIZES = (192, 256, 256, 192, 128)
 SIDE = 4
 F32 = jnp.float32
 BF16 = jnp.bfloat16
@@ -16,14 +16,14 @@
 SETS = {"V": "x", "U": "x", "O": "y", "D": "y", "G": "z"}
 RING = {"H": 1, "I": 1, "r1": 1, "r2": 1}
 FAR = {"p": "pp", "m": "mm"}
-POOL = 40
-RECEIVES = 94
+POOL = 32
+RECEIVES = 116
 
 
 def slot_of(key):
     name = key[0]
     if name in SETS:
-        return (SETS[name], *key[1:])
+        return (SETS[name] if key[2] > 2 else name, *key[1:])
     if name in RING and key[2] != "c":
         return ("ring", key[1], FAR[key[2]] if name == "r2" else key[2])
     return key
@@ -70,7 +70,8 @@
     send_sems, recv_sems, local_sems,
 ):
     length = nb.shape[0]
-    rows = length // CHUNKS
+    rows = length // SIDE
+    starts = [sum(SIZES[:c]) for c in range(len(SIZES))]
     model = nb.shape[1]
     width = heads.shape[1] // 8
     cols = hid.shape[1] // 8
@@ -116,22 +117,6 @@
     load("g", gate_hbm, gbuf.at[z, x])
     half_o, half_f = out_hbm.shape[0] // 2, fg_hbm.shape[0] // 2
     quarter = down_hbm.shape[0] // 4
-    for c in range(CHUNKS):
-        load(("tok", c), tok_hbm.at[0, pl.ds(c * rows, rows)], tok.at[pl.ds(c * rows, rows)])
-        if c == 0:
-            for u in range(2):
-                load(("O", u), out_hbm.at[pl.ds(u * half_o, half_o)], obuf.at[z, x, u])
-    for u in range(2):
-        load(("G", u), fg_hbm.at[pl.ds(u * half_f, half_f)], fgbuf.at[z, x, u])
-        load(("U", u), fu_hbm.at[pl.ds(u * half_f, half_f)], fubuf.at[z, x, u])
-        mine = pl.multiple_of(u * half_f + core * quarter, quarter)
-        load(("D", u), down_hbm.at[pl.ds(mine, quarter)], dbuf.at[u, z, x, core])
-
-    tapf[pl.ds(0, taps.shape[0])] = taps[...].astype(F32)
-    fftapf[pl.ds(0, fftaps.shape[0])] = fftaps[...].astype(F32)
-    glu[pl.ds(0, 32)] = jnp.zeros((32, glu.shape[1]), F32)
-    ffg[pl.ds(0, 8)] = jnp.zeros((8, units), F32)
-
     net = Exchange(send_sems, recv_sems)
 
     def pick_v(u, zi, xi, h=None):
@@ -179,8 +164,9 @@
         relay((n, u, 2, "m"), near(n, u, 1, 1), first_ring[u][1])
 
     def s3(n, u):
-        net.got((n, u, 2, "p"))
-        net.got((n, u, 2, "m"))
+        for v in {"U": (0, 1), "D": (0, 1)}.get(n, (u,)) if u == 0 or n not in "UD" else ():
+            net.got((n, v, 2, "p"))
+            net.got((n, v, 2, "m"))
         plus, minus = second_ring[u]
         relay((n, u, 3, "p0"), block(n, u, 0, 0), plus)
         relay((n, u, 3, "m0"), block(n, u, 0, 1), minus)
@@ -203,8 +189,8 @@
         net.got((n, u, 4, "m"))
 
     def chunk_ref(buf, wide, c, d, h=None):
-        count = rows if h is None else rows // 2
-        start = c * rows + (0 if h is None else h * count)
+        count = SIZES[c] if h is None else SIZES[c] // 2
+        start = starts[c] + (0 if h is None else h * count)
         lane = pl.multiple_of(core * SIDE * wide + around(y, d) * wide, wide)
         return buf.at[pl.ds(start, count), pl.ds(lane, wide)]
 
@@ -223,38 +209,38 @@
         net.got((n, c, "pp"))
         net.got((n, c, "mm"))
         lane = pl.multiple_of(core * SIDE * wide, SIDE * wide)
-        relay((n, c, "c"), buf.at[pl.ds(c * rows, rows), pl.ds(lane, SIDE * wide)], partner)
+        relay((n, c, "c"), buf.at[pl.ds(starts[c], SIZES[c]), pl.ds(lane, SIDE * wide)], partner)
 
     def a4(n, c):
         net.got((n, c, "c"))
 
-    def norm(src, gain, c, starts):
-        few, wide = 16, model // len(starts)
+    def norm(src, gain, first, count, lanes):
+        few, wide = 16, model // len(lanes)
 
         def body(i, _):
-            at = pl.ds(pl.multiple_of(c * rows + i * few, few), few)
-            parts = [src[at, pl.ds(start, wide)] for start in starts]
+            at = pl.ds(pl.multiple_of(first + i * few, few), few)
+            parts = [src[at, pl.ds(start, wide)] for start in lanes]
             value = jnp.concatenate(parts, axis=1).astype(F32)
             scale = lax.rsqrt(jnp.mean(value * value, axis=-1, keepdims=True) + FLOOR)
             nb[at] = (value * scale * gain[...].astype(F32).reshape(1, model)).astype(BF16)
             return 0
 
-        lax.fori_loop(0, rows // few, body, 0, unroll=4)
+        lax.fori_loop(0, count // few, body, 0, unroll=4)
 
     def mixa(c):
-        at = pl.ds(c * rows, rows)
+        at = pl.ds(starts[c], SIZES[c])
         both = jnp.concatenate(
             [vbuf[...].reshape(model, width), gbuf[...].reshape(model, width)], axis=1
         )
         pair = jnp.dot(nb[at], both, preferred_element_type=F32)
-        glu[pl.ds(32 + c * rows, rows)] = pair[:, :width] * jax.nn.sigmoid(pair[:, width:])
+        glu[pl.ds(32 + starts[c], SIZES[c])] = pair[:, :width] * jax.nn.sigmoid(pair[:, width:])
 
     def mix(c):
         few, count = 64, taps.shape[0]
         lead = 32 - (count - 1)
 
         def body(i, _):
-            base = pl.multiple_of(c * rows + i * few, few)
+            base = pl.multiple_of(starts[c] + i * few, few)
             total = None
             for r in range(8):
                 part = None
@@ -273,10 +259,10 @@
             heads[pl.ds(base, few), lanes] = jax.nn.silu(normal).astype(BF16)
             return 0
 
-        lax.fori_loop(0, rows // few, body, 0)
+        lax.fori_loop(0, SIZES[c] // few, body, 0)
 
     def hidden(c):
-        at = pl.ds(c * rows, rows)
+        at = pl.ds(starts[c], SIZES[c])
         lanes = pl.ds(pl.multiple_of(tp * cols, cols), cols)
         mine = pl.ds(pl.multiple_of(core * SIDE * cols + y * cols, cols), cols)
         weight = jnp.concatenate(
@@ -286,12 +272,12 @@
         hid[at, mine] = (tok[at, lanes].astype(F32) + total).astype(BF16)
 
     def gate(c, n):
-        at, lanes = pl.ds(c * rows, rows), pl.ds(n * step, step)
+        at, lanes = pl.ds(starts[c], SIZES[c]), pl.ds(n * step, step)
         weight = fgbuf[:, :, :, :, lanes].reshape(model, step)
-        ffg[pl.ds(8 + c * rows, rows), lanes] = jnp.dot(nb[at], weight, preferred_element_type=F32)
+        ffg[pl.ds(8 + starts[c], SIZES[c]), lanes] = jnp.dot(nb[at], weight, preferred_element_type=F32)
         few = 32
-        for i in range(rows // few):
-            base = c * rows + i * few
+        for i in range(SIZES[c] // few):
+            base = starts[c] + i * few
             seen = ffg[pl.ds(base, few + 8), lanes]
             total = seen[6 : 6 + few] * fftapf[pl.ds(0, 1), lanes]
             total = total + seen[7 : 7 + few] * fftapf[pl.ds(1, 1), lanes]
@@ -398,40 +384,60 @@
         for u in range(2):
             net.got(("d", u))
 
+    def loads():
+        for c in range(SIDE):
+            load(("tok", c), tok_hbm.at[0, pl.ds(c * rows, rows)], tok.at[pl.ds(c * rows, rows)])
+            if c == 0:
+                for u in range(2):
+                    load(("O", u), out_hbm.at[pl.ds(u * half_o, half_o)], obuf.at[z, x, u])
+        for u in range(2):
+            load(("G", u), fg_hbm.at[pl.ds(u * half_f, half_f)], fgbuf.at[z, x, u])
+            load(("U", u), fu_hbm.at[pl.ds(u * half_f, half_f)], fubuf.at[z, x, u])
+            mine = pl.multiple_of(u * half_f + core * quarter, quarter)
+            load(("D", u), down_hbm.at[pl.ds(mine, quarter)], dbuf.at[u, z, x, core])
+
+    def tables():
+        tapf[pl.ds(0, taps.shape[0])] = taps[...].astype(F32)
+        fftapf[pl.ds(0, fftaps.shape[0])] = fftaps[...].astype(F32)
+        glu[pl.ds(0, 32)] = jnp.zeros((32, glu.shape[1]), F32)
+        ffg[pl.ds(0, 8)] = jnp.zeros((8, units), F32)
+
     def normed(c):
         ready(("tok", c))
-        norm(tok, mixg, c, [0])
+        norm(tok, mixg, c * rows, rows, [0])
 
     def renormed(c):
-        norm(hid, ffng, c, in_order)
+        norm(hid, ffng, starts[c], SIZES[c], in_order)
 
     def meet():
         pl.semaphore_wait(barrier, len(peers))
 
     for step_of, *given in (
-        (normed, 0), (normed, 1), (meet,), (s1, "V", 0), (s1, "V", 1), (halves,), (halves_in,),
-        (normed, 2), (normed, 3), (s2, "V", 0), (s2, "V", 1), (s1, "O", 0), (s1, "O", 1), (s1, "G", 0),
-        (s1, "G", 1), (s3, "V", 0), (s3, "V", 1), (s2, "O", 0), (s2, "O", 1), (s2, "G", 0), (s2, "G", 1),
-        (s4, "V", 0), (s4, "V", 1), (s5, "V", 0), (s5, "V", 1), (s3, "O", 0), (s3, "O", 1), (s3, "G", 0),
-        (s3, "G", 1), (s6, "V", 0), (s6, "V", 1), (s1, "U", 0), (s1, "U", 1), (mixa, 0), (mix, 0),
-        (a1, *H, 0), (s4, "O", 0), (s4, "O", 1), (s5, "O", 0), (s5, "O", 1), (mixa, 1), (mix, 1),
-        (a1, *H, 1), (mixa, 2), (mix, 2), (a1, *H, 2), (mixa, 3), (s4, "G", 0), (s4, "G", 1), (mix, 3),
-        (a2, *H, 0), (a1, *H, 3), (a2, *H, 1), (a2, *H, 2), (s5, "G", 0), (s5, "G", 1), (a3, *H, 0),
-        (a2, *H, 3), (a4, "H", 0), (s2, "U", 0), (s2, "U", 1), (a3, *H, 1), (s6, "O", 0), (s6, "O", 1),
-        (s1, "D", 0), (s1, "D", 1), (hidden, 0), (a3, *H, 2), (a1, *I, 0), (a4, "H", 1), (hidden, 1),
-        (a1, *I, 1), (a4, "H", 2), (hidden, 2), (a3, *H, 3), (a4, "H", 3), (hidden, 3), (s6, "G", 0),
-        (s6, "G", 1), (s3, "U", 0), (s3, "U", 1), (a2, *I, 0), (a1, *I, 2), (s2, "D", 0), (s2, "D", 1),
-        (a2, *I, 1), (a1, *I, 3), (a3, *I, 0), (a4, "I", 0), (renormed, 0), (s4, "U", 0), (s4, "U", 1),
-        (gate, 0, 0), (a2, *I, 2), (gate, 0, 1), (gate, 0, 2), (a3, *I, 1), (s5, "U", 0), (s5, "U", 1),
-        (a4, "I", 1), (renormed, 1), (a2, *I, 3), (gate, 1, 0), (s3, "D", 0), (s3, "D", 1), (gate, 1, 1),
-        (a3, *I, 2), (gate, 1, 2), (a4, "I", 2), (renormed, 2), (gate, 2, 0), (a3, *I, 3), (s6, "U", 0),
-        (s6, "U", 1), (gate, 2, 1), (gate, 2, 2), (a4, "I", 3), (renormed, 3), (gate, 3, 0), (gate, 3, 1),
-        (gate, 3, 2), (s4, "D", 0), (s4, "D", 1), (up, 2, 0), (up, 2, 1), (up, 2, 2), (up, 1, 0),
-        (up, 1, 1), (up, 1, 2), (up, -1, 0), (up_in, 2), (ra, 0), (s5, "D", 0), (s5, "D", 1), (ra, 1),
-        (ra, 2), (up_in, 1), (up, -1, 1), (up, -1, 2), (up, 0, 0), (up, 0, 1), (up, 0, 2), (up_in, -1),
-        (rb, 0), (s6, "D", 0), (s6, "D", 1), (rc, 0), (ra, 3), (rb, 1), (up_in, 0), (rc, 1), (rd, 0),
-        (rd, 1), (rb, 2), (rc, 2), (rd, 2), (rb, 3), (rd, 3), (re, 0), (rc, 3), (rf, 0), (re, 1), (rf, 1),
-        (re, 2), (rf, 2), (re, 3), (rf, 3),
+        (loads,), (meet,), (s1, "V", 0), (s1, "V", 1), (tables,), (s1, "O", 0), (s1, "O", 1), (halves,),
+        (s1, "G", 0), (s1, "G", 1), (normed, 0), (normed, 1), (halves_in,), (normed, 2), (normed, 3),
+        (s2, "V", 0), (s2, "V", 1), (s1, "U", 0), (s1, "U", 1), (s2, "O", 0), (s2, "O", 1), (s2, "G", 0),
+        (s2, "G", 1), (s3, "V", 0), (s3, "V", 1), (s3, "O", 0), (s3, "O", 1), (s4, "V", 0), (s4, "V", 1),
+        (s3, "G", 0), (s3, "G", 1), (s1, "D", 0), (s1, "D", 1), (s5, "V", 0), (s5, "V", 1), (s4, "O", 0),
+        (s4, "O", 1), (s5, "O", 0), (s5, "O", 1), (s6, "V", 0), (s6, "V", 1), (s2, "U", 0), (s2, "U", 1),
+        (mixa, 0), (mix, 0), (a1, *H, 0), (mixa, 1), (mix, 1), (a1, *H, 1), (mixa, 2), (mix, 2),
+        (a1, *H, 2), (s4, "G", 0), (s4, "G", 1), (mixa, 3), (a2, *H, 0), (mix, 3), (a1, *H, 3), (mixa, 4),
+        (mix, 4), (a1, *H, 4), (a2, *H, 1), (s5, "G", 0), (s5, "G", 1), (a2, *H, 2), (a3, *H, 0),
+        (a2, *H, 3), (a4, "H", 0), (a2, *H, 4), (s6, "O", 0), (s6, "O", 1), (hidden, 0), (a1, *I, 0),
+        (a3, *H, 1), (s3, "U", 0), (s3, "U", 1), (s2, "D", 0), (s2, "D", 1), (a3, *H, 2), (a4, "H", 1),
+        (hidden, 1), (a1, *I, 1), (a3, *H, 3), (a4, "H", 2), (hidden, 2), (a3, *H, 4), (a4, "H", 3),
+        (hidden, 3), (a4, "H", 4), (hidden, 4), (a2, *I, 0), (a1, *I, 2), (s6, "G", 0), (s6, "G", 1),
+        (a2, *I, 1), (a1, *I, 3), (a3, *I, 0), (s4, "U", 0), (s4, "U", 1), (a4, "I", 0), (renormed, 0),
+        (gate, 0, 0), (gate, 0, 1), (a2, *I, 2), (a1, *I, 4), (gate, 0, 2), (a3, *I, 1), (s5, "U", 0),
+        (s5, "U", 1), (s3, "D", 0), (s3, "D", 1), (a4, "I", 1), (renormed, 1), (a2, *I, 3), (gate, 1, 0),
+        (gate, 1, 1), (a3, *I, 2), (gate, 1, 2), (a2, *I, 4), (a4, "I", 2), (renormed, 2), (s6, "U", 0),
+        (s6, "U", 1), (gate, 2, 0), (a3, *I, 3), (gate, 2, 1), (gate, 2, 2), (a4, "I", 3), (renormed, 3),
+        (a3, *I, 4), (gate, 3, 0), (gate, 3, 1), (gate, 3, 2), (s4, "D", 0), (s4, "D", 1), (a4, "I", 4),
+        (renormed, 4), (gate, 4, 0), (gate, 4, 1), (gate, 4, 2), (up, 2, 0), (up, 2, 1), (up, 2, 2),
+        (up, 1, 0), (up, 1, 1), (up, 1, 2), (up, -1, 0), (up, -1, 1), (up_in, 2), (s5, "D", 0),
+        (s5, "D", 1), (ra, 0), (ra, 1), (ra, 2), (up_in, 1), (up, -1, 2), (up, 0, 0), (up, 0, 1),
+        (up, 0, 2), (up_in, -1), (rb, 0), (s6, "D", 0), (s6, "D", 1), (ra, 3), (up_in, 0), (rd, 0),
+        (rc, 0), (rb, 1), (rc, 1), (rd, 1), (rb, 2), (rc, 2), (rd, 2), (rb, 3), (rc, 3), (rd, 3), (re, 0),
+        (rf, 0), (re, 1), (rf, 1), (re, 2), (rf, 2), (re, 3), (rf, 3),
     ):
         tag = "_".join(str(part) for part in given if isinstance(part, (int, str)))
         with jax.named_scope(step_of.__name__ + "_" + tag):
@@ -466,7 +472,7 @@
     _, length, model = tokens.shape
     width, cols, units = value_weight.shape[1], out_weight.shape[1], ffgate_weight.shape[1]
     deep, deep_o, deep_d = value_weight.shape[0], out_weight.shape[0], down_weight.shape[0]
-    rows, positions, part = length // CHUNKS, length // 8, 2 * deep_d
+    rows, positions, part = length // SIDE, length // 8, 2 * deep_d
     vmem = pl.BlockSpec(memory_space=pltpu.VMEM)
     hbm = pl.BlockSpec(memory_space=pl.ANY)
     four = (SIDE, SIDE)

time: 95.3 us -> 91.9 us (0.964)
  Pallas kernels: 93.2 us -> 89.8 us
    pallas_call x1, Pallas kernels: 93.2 us -> 89.8 us  [on_device(): pl.pallas_call(kernel, out_shape=jax.ShapeDtypeStruct((1, positions, mode...]
where the time goes in v3:
time: 91.9 us; the launch traced here: 91.7 us
  Pallas kernels  89.8 us (98%)
  local copies, waits for them, and re-layouts  1.88 us (2%)
    pallas_call x1, Pallas kernels, on_device(): pl.pallas_call(kernel, out_shape=jax.ShapeDtypeStruct((1, positions, mode...  89.8 us
    unnamed x1, local copies, waits for them, and re-layouts  1.88 us

profile of v3, /device:TPU:1, one launch (start us, length us, event | category | flops | bytes accessed | tf_op | source)
XLA Modules:
  0.0 91.7 jit_solution(1680560894941083009)
XLA Ops:
  0.0 89.8 %layer.1 = bf16[1,128,2048]{2,1,0:T(8,128)(2,1)} custom-call(bf16[1,1024,2048]{2,1,0:T(8,128)(2,1)} %tok_hbm.1, bf16[2048]{0:T(1024)(128)(2,1)} %mixg.1, bf16[128,128]{1,0:T(8,128)(2,1)} %value_hbm.1, bf16[128,128]{1,0:T(8,128)(2,1)} %gate_hbm.1, bf16[31,128]{1,0:T(8,128)(2,1)} %taps.1, bf16[1,128]{1,0:T(2,128)(2,1)} %bitcast.1, bf16[64,256]{1,0:T(8,128)(2,1)} %out_hbm.1, ...), custom_call_target="tpu_custom_call" | custom-call | tf_op jit(solution)/shard_map/layer/pallas_call | solution.py:512
  89.8 1.9 %copy.14 = bf16[1,128,2048]{2,1,0:T(8,128)(2,1)} copy(bf16[1,128,2048]{2,1,0:T(8,128)(2,1)} %layer.1) | data formatting | bytes 1048576

commit v4 on v3

--- a/solution.py
+++ b/solution.py
@@ -16,7 +16,7 @@
 SETS = {"V": "x", "U": "x", "O": "y", "D": "y", "G": "z"}
 RING = {"H": 1, "I": 1, "r1": 1, "r2": 1}
 FAR = {"p": "pp", "m": "mm"}
-POOL = 32
+POOL = 56
 RECEIVES = 116
 
 

time: 91.9 us -> 92 us (level)
  no operation moved by 1% of the time
where the time goes in v4:
time: 92 us; the launch traced here: 91.9 us
  Pallas kernels  90 us (98%)
  local copies, waits for them, and re-layouts  1.88 us (2%)
    pallas_call x1, Pallas kernels, on_device(): pl.pallas_call(kernel, out_shape=jax.ShapeDtypeStruct((1, positions, mode...  90 us
    unnamed x1, local copies, waits for them, and re-layouts  1.88 us

profile of v4, /device:TPU:1, one launch (start us, length us, event | category | flops | bytes accessed | tf_op | source)
XLA Modules:
  0.0 91.9 jit_solution(18285785607608057997)
XLA Ops:
  0.0 90.0 %layer.1 = bf16[1,128,2048]{2,1,0:T(8,128)(2,1)} custom-call(bf16[1,1024,2048]{2,1,0:T(8,128)(2,1)} %tok_hbm.1, bf16[2048]{0:T(1024)(128)(2,1)} %mixg.1, bf16[128,128]{1,0:T(8,128)(2,1)} %value_hbm.1, bf16[128,128]{1,0:T(8,128)(2,1)} %gate_hbm.1, bf16[31,128]{1,0:T(8,128)(2,1)} %taps.1, bf16[1,128]{1,0:T(2,128)(2,1)} %bitcast.1, bf16[64,256]{1,0:T(8,128)(2,1)} %out_hbm.1, ...), custom_call_target="tpu_custom_call" | custom-call | tf_op jit(solution)/shard_map/layer/pallas_call | solution.py:512
  90.0 1.9 %copy.14 = bf16[1,128,2048]{2,1,0:T(8,128)(2,1)} copy(bf16[1,128,2048]{2,1,0:T(8,128)(2,1)} %layer.1) | data formatting | bytes 1048576
